TPU v7x, 512 devices: a whole 4x8x8 slice. The times are simulated.
512 devices in a mesh: ep: 32 (over z, x), tp: 16 (over y, core).
Axes of the slice: x: 4, y: 8, z: 8, core: 2. Of those that a mesh axis runs over, the one named last changes fastest.
Arguments:
- queries: bfloat16 [196608, 1024], P(('ep', 'tp')), may hold values from -250 to 250
- keys_values: bfloat16 [2, 196608, 256], P(None, ('ep', 'tp')), may hold values from -8 to 8
- sink_logits: float32 [16], replicated, may hold values from 2 to 6
- moe_rows: bfloat16 [8192, 2048], P('ep'), may hold values from -600 to 600
- norm_gain: float32 [2048], replicated, may hold values from 0.1 to 1.9
- group_choice: int32 [8192], P('ep'), may hold values from 0 to 7, as said below
- member_choice: int32 [8192, 2], P('ep'), may hold values from 0 to 3, as said below
- route_weight: float32 [8192, 2], P('ep'), may hold values from 0.1 to 1
- w_gate: bfloat16 [32, 2048, 2048], P('ep', None, 'tp'), may hold values from -0.125 to 0.125
- w_up: bfloat16 [32, 2048, 2048], P('ep', None, 'tp'), may hold values from -0.125 to 0.125
- w_down: bfloat16 [32, 2048, 2048], P('ep', None, 'tp'), may hold values from -0.125 to 0.125
Outputs:
- attended: bfloat16 [196608, 1024], P(('ep', 'tp'))
- mixed: bfloat16 [8192, 2048], P('ep', 'tp')
Inputs may be any that keep to these rules, and one draw needn't show every extreme that they name: With expert = group_choice * 4 + member_choice, within the 256 rows of one index of ep no expert is named by more than 32 rows, and some expert is named by exactly 32 rows. `member_choice`: the 2 entries of a row differ.
All inputs are finite; a program needn't handle non-finite values.
Results may differ from a plain program's by a relative error of at most 0.007.
Values may be sent and summed in bfloat16 or wider, within the bound.
A program may use at most 64 MiB of HBM per device.

v0:
```python
import jax
import jax.numpy as jnp
from jax import lax
from jax.sharding import PartitionSpec as P

QH = 16
KVH = 4
HD = 64
WINDOW = 128
EPG = 4
TOP = 2


def passed_along(value, axis, by):
    peers = lax.axis_size(axis)
    pairs = [(i, i + by) for i in range(peers) if 0 <= i + by < peers]
    return lax.ppermute(value, axis, pairs)


def attend_window(queries, keys_values, sink_logits):
    length = queries.shape[0]
    sharing = QH // KVH
    blocks = length // WINDOW
    edge_rows = keys_values[:, length - WINDOW :, :]
    earlier_keys = passed_along(edge_rows, ("ep", "tp"), 1)
    joined = jnp.concatenate([earlier_keys, keys_values], axis=1)
    first_half = joined[:, :length].reshape(2, blocks, WINDOW, KVH, HD)
    second_half = joined[:, WINDOW:].reshape(2, blocks, WINDOW, KVH, HD)
    banded = jnp.concatenate([first_half, second_half], axis=2)
    query_blocks = queries.reshape(blocks, WINDOW, KVH, sharing, HD)
    scores = jnp.einsum(
        "bqhgd,bkhd->bhgqk", query_blocks, banded[0], preferred_element_type=jnp.float32
    ) * HD ** (-0.5)
    offset = lax.axis_index(("ep", "tp")) * length
    key_column = jnp.arange(2 * WINDOW, dtype=jnp.int32)
    distance = jnp.arange(WINDOW, dtype=jnp.int32)[:, None] + WINDOW - key_column[None, :]
    inside = (distance >= 0) & (distance < WINDOW)
    key_position = (
        offset
        + jnp.arange(blocks, dtype=jnp.int32)[:, None] * WINDOW
        + key_column[None, :]
        - WINDOW
    )
    visible = inside[None, :, :] & (key_position[:, None, :] >= 0)
    scores = jnp.where(visible[:, None, None, :, :], scores, -1e30)
    sink_column = sink_logits.reshape(KVH, sharing)[None, :, :, None]
    highest = jnp.maximum(jnp.max(scores, axis=-1), sink_column)
    weights = jnp.exp(scores - highest[..., None])
    totals = jnp.sum(weights, axis=-1) + jnp.exp(sink_column - highest)
    summed = jnp.einsum(
        "bhgqk,bkhd->bqhgd",
        weights.astype(jnp.bfloat16),
        banded[1],
        preferred_element_type=jnp.float32,
    )
    attended = summed / jnp.transpose(totals, (0, 3, 1, 2))[..., None]
    return attended.astype(jnp.bfloat16).reshape(length, QH * HD)


def route_experts(
    moe_rows, norm_gain, group_choice, member_choice, route_weight, w_gate, w_up, w_down
):
    token_count = moe_rows.shape[0]
    row_width = moe_rows.shape[1]
    ep_count = lax.axis_size("ep")
    local_experts = w_gate.shape[0]
    expert_count = ep_count * local_experts
    capacity = 2 * TOP * token_count // expert_count
    values = moe_rows.astype(jnp.float32)
    normed = (
        values * lax.rsqrt(jnp.mean(values * values, axis=1, keepdims=True) + 1e-06) * norm_gain
    ).astype(jnp.bfloat16)
    chosen = (group_choice[:, None] * EPG + member_choice).reshape(-1)
    onehot = (chosen[:, None] == jnp.arange(expert_count, dtype=jnp.int32)[None, :]).astype(
        jnp.int32
    )
    earlier = jnp.cumsum(onehot, axis=0) - onehot
    destination = chosen * capacity + jnp.sum(earlier * onehot, axis=1)
    source_row = jnp.arange(token_count * TOP, dtype=jnp.int32) // TOP
    lookup = (
        jnp.full((expert_count * capacity,), token_count, jnp.int32).at[destination].set(source_row)
    )
    padded = jnp.concatenate([normed, jnp.zeros((1, row_width), jnp.bfloat16)], axis=0)
    share_count = capacity // lax.axis_size("tp")
    slot_table = lookup.reshape(expert_count, capacity)
    my_slots = lax.dynamic_slice_in_dim(
        slot_table, lax.axis_index("tp") * share_count, share_count, 1
    )
    outgoing = padded[my_slots.reshape(-1)].reshape(ep_count, local_experts, share_count, row_width)
    incoming = lax.all_to_all(outgoing, "ep", split_axis=0, concat_axis=0, tiled=True)
    block_rows = lax.all_gather(incoming, "tp", axis=2, tiled=True)
    gate_part = jnp.einsum("secd,edf->secf", block_rows, w_gate, preferred_element_type=jnp.float32)
    up_part = jnp.einsum("secd,edf->secf", block_rows, w_up, preferred_element_type=jnp.float32)
    hidden = (jax.nn.silu(gate_part) * up_part).astype(jnp.bfloat16)
    out_width = w_down.shape[2]
    produced = jnp.einsum(
        "secf,efd->secd",
        lax.all_gather(hidden, "tp", axis=3, tiled=True),
        w_down,
        preferred_element_type=jnp.float32,
    )
    produced = produced.astype(jnp.bfloat16).reshape(ep_count, local_experts * capacity, out_width)
    returned = lax.all_to_all(produced, "ep", split_axis=0, concat_axis=0, tiled=True)
    picked = returned.reshape(expert_count * capacity, out_width)[destination]
    picked = picked.reshape(token_count, TOP, out_width).astype(jnp.float32)
    return jnp.sum(route_weight[:, :, None] * picked, axis=1).astype(jnp.bfloat16)


def shards(
    queries,
    keys_values,
    sink_logits,
    moe_rows,
    norm_gain,
    group_choice,
    member_choice,
    route_weight,
    w_gate,
    w_up,
    w_down,
):
    attended = attend_window(queries, keys_values, sink_logits)
    mixed = route_experts(
        moe_rows, norm_gain, group_choice, member_choice, route_weight, w_gate, w_up, w_down
    )
    return (attended, mixed)


def solution(mesh):
    in_specs = (
        P(("ep", "tp"), None),
        P(None, ("ep", "tp"), None),
        P(),
        P("ep", None),
        P(),
        P("ep"),
        P("ep", None),
        P("ep", None),
        P("ep", None, "tp"),
        P("ep", None, "tp"),
        P("ep", None, "tp"),
    )
    out_specs = (P(("ep", "tp"), None), P("ep", "tp"))
    return jax.shard_map(shards, mesh=mesh, in_specs=in_specs, out_specs=out_specs, check_vma=False)
```

profile of v0, /device:TPU:1, one launch (start us, length us, event | category | flops | bytes accessed | tf_op | source)
XLA Modules:
  0.0 180.1 jit_solution(10579058305532520949)
XLA Ops:
  7.2 0.7 broadcast_multiply_fusion.1
  8.0 0.7 broadcast_multiply_fusion
  9.1 1.2 reduce-window.6
  10.3 0.2 slice_reduce_fusion
  11.0 2.4 %scatter_custom_fusion = s32[1024]{0:T(1024)S(1)} fusion(s32[512]{0:T(512)S(1)} %bitcast.107, s32[512]{0:T(512)S(1)} %add_select_fusion, s32[]{:T(128)} %constant.66.clone.1), kind=kCustom, calls=%fused_computation.75 | custom fusion | bytes 4100 | tf_op jit(solution)/shard_map/scatter | solution.py:81
  13.7 1.5 fusion.17
  15.2 1.5 fusion.19
  16.8 0.7 gather_fusion
  17.8 24.9 %all_to_all.10 = bf16[32,1,2,2048]{3,2,1,0:T(2,128)(2,1)S(1)} all-to-all(bf16[32,1,2,2048]{3,2,1,0:T(2,128)(2,1)S(1)} %bitcast.105), channel_id=1, replica_groups=mesh['ep'=32,'tp'=16] {'ep'}, dimensions={0} | all-to-all | bytes 524288 | tf_op jit(solution)/shard_map/all_to_all | solution.py:90
  42.7 0.8 copy.44
  43.6 42.1 %all-gather.3.cloned.1.call-done = bf16[32,1,32,2048]{3,0,1,2:T(8,128)(2,1)} async-done(((bf16[32,1,2,2048]{3,0,1,2:T(8,128)(2,1)}), bf16[32,1,32,2048]{3,0,1,2:T(8,128)(2,1)}) %all-gather.3.cloned.1.call-update) | async-done | bytes 4194320 | tf_op jit(solution)/shard_map/all_gather | solution.py:91
  85.7 5.2 %fusion.25 = f32[32,1,32,128]{3,2,0,1:T(8,128)S(1)} fusion(bf16[32,1,32,2048]{3,0,1,2:T(8,128)(2,1)} %all-gather.3.cloned.1.call-done, bf16[1,2048,128]{2,1,0:T(8,128)(2,1)S(1)} %copy-done), kind=kOutput, calls=%fused_computation.30 | convolution fusion | flops 536870912 | bytes 5242880 | tf_op jit(solution)/shard_map/secd,edf->secf/dot_general | solution.py:92
  90.9 3.6 %fusion.34 = bf16[32,1,32,128]{3,2,0,1:T(8,128)(2,1)} fusion(bf16[32,1,32,2048]{3,0,1,2:T(8,128)(2,1)S(1)} %copy-done.6, bf16[1,2048,128]{2,1,0:T(8,128)(2,1)S(1)} %copy-done.7, f32[32,1,32,128]{3,2,0,1:T(8,128)S(1)} %fusion.25), kind=kOutput, calls=%fused_computation.33 | convolution fusion | flops 537657344 | bytes 5505024 | tf_op jit(solution)/shard_map/secd,edf->secf/dot_general | solution.py:93
  94.6 3.3 %collective-permute-start = (bf16[2,128,256]{2,1,0:T(8,128)(2,1)S(1)}, bf16[2,128,256]{2,1,0:T(8,128)(2,1)S(1)}, u32[]{:S(2)}, u32[]{:S(2)}) collective-permute-start(bf16[2,128,256]{2,1,0:T(8,128)(2,1)S(1)} %slice.18), channel_id=1, source_target_pairs={{0,1},{1,2},{2,3},{3,4},{4,5},{5,6},{6,7},{7,8},{8,9},{9,10},{10,1... | collective-permute-start | bytes 393224 | tf_op jit(solution)/shard_map/ppermute | solution.py:17
  98.3 0.3 reshape.243
  98.6 0.5 copy.33
  99.1 3.4 %reshape.244 = bf16[3,128,4,4,64]{4,3,2,1,0:T(4,128)(2,1)S(1)} reshape(bf16[384,1024]{1,0:T(8,128)(2,1)} %param.11) | data formatting | bytes 1572864 | tf_op jit(solution)/shard_map/reshape | solution.py:30
  102.7 0.8 pad_maximum_fusion.1
  103.5 1.8 %reshape.242 = bf16[2,3,128,4,64]{4,3,2,1,0:T(4,128)(2,1)S(1)} reshape(bf16[2,384,256]{2,1,0:T(8,128)(2,1)} %pad_maximum_fusion.1) | data formatting | bytes 786432 | tf_op jit(solution)/shard_map/reshape | solution.py:27
  105.3 1.1 copy.32
  106.4 2.2 %fusion.2 = (f32[3,4,4,128]{3,2,1,0:T(4,128)S(1)}, f32[3,4,256,128,4]{3,2,4,1,0:T(8,128)S(1)}) fusion(pred[3,128,256]{1,2,0:T(8,128)(4,1)S(1)} %broadcast_and_fusion, bf16[3,128,4,4,64]{4,3,2,1,0:T(4,128)(2,1)S(1)} %reshape.244, bf16[2,3,128,4,64]{2,4,3,1,0:T(8,128)(2,1)S(1)} %copy.33, bf16[2,3,128,4,64]{2,4,3,1,0:T(8,128)(2,1)} %copy.32), kind=kOutput, calls=%fused_computation.7 | convolution fusion | flops 206825472 | bytes 7987200 | tf_op jit(solution)/shard_map/bqhgd,bkhd->bhgqk/dot_general | solution.py:31
  108.7 2.6 %copy-done.1 = f32[3,4,256,128,4]{3,2,4,1,0:T(8,128)} copy-done((f32[3,4,256,128,4]{3,2,4,1,0:T(8,128)}, f32[3,4,256,128,4]{3,2,4,1,0:T(8,128)S(1)}, u32[]{:S(2)}) %copy-start.1) | copy-done | bytes 6291480
  111.3 1.6 fusion
  113.0 33.0 %all-gather.5.cloned.1.call-done = bf16[32,1,32,2048]{3,2,0,1:T(8,128)(2,1)} async-done(((bf16[32,1,32,128]{3,2,0,1:T(8,128)(2,1)}), bf16[32,1,32,2048]{3,2,0,1:T(8,128)(2,1)}) %all-gather.5.cloned.1.call-update) | async-done | bytes 4194320 | tf_op jit(solution)/shard_map/all_gather | solution.py:98
  146.0 4.2 %fusion.37 = bf16[32,32,128]{2,1,0:T(8,128)(2,1)} fusion(bf16[32,1,32,2048]{3,2,0,1:T(8,128)(2,1)} %all-gather.5.cloned.1.call-done, bf16[1,2048,128]{2,1,0:T(8,128)(2,1)S(1)} %copy-done.8), kind=kOutput, calls=%fused_computation.34 | convolution fusion | flops 537001984 | bytes 4980736 | tf_op jit(solution)/shard_map/secf,efd->secd/dot_general | solution.py:96
  150.2 8.9 %all-to-all-start.1 = ((bf16[32,32,128]{2,1,0:T(8,128)(2,1)}), bf16[32,32,128]{2,1,0:T(8,128)(2,1)S(1)}, u32[]{:S(2)}, u32[]{:S(2)}) async-start(bf16[32,32,128]{2,1,0:T(8,128)(2,1)} %fusion.37), calls=%async_computation.1 | async-start | bytes 524288 | tf_op jit(solution)/shard_map/all_to_all | solution.py:103
  159.1 5.2 %fusion.20 = bf16[3,128,4,4,64]{1,4,3,2,0:T(8,128)(2,1)} fusion(f32[3,4,256,128,4]{3,2,4,1,0:T(8,128)} %copy-done.1, f32[3,4,4,128]{3,2,1,0:T(4,128)S(1)} %broadcast_maximum_fusion, pred[3,128,256]{1,2,0:T(8,128)(4,1)S(1)} %broadcast_and_fusion, f32[3,128,4,4]{1,3,2,0:T(4,128)S(1)} %add_bitcast_fusion.1, bf16[2,3,128,4,64]{2,4,3,1,0:T(8,128)(2,1)S(1)} %copy-done.3, ...), kind=kOutput, calls=%fused_computation.27 | convolution fusion | flops 209190912 | bytes 8011776 | tf_op jit(solution)/shard_map/bhgqk,bkhd->bqhgd/dot_general | solution.py:50
  164.4 2.8 %copy.56 = bf16[3,128,4,4,64]{4,3,2,1,0:T(4,128)(2,1)S(1)} copy(bf16[3,128,4,4,64]{1,4,3,2,0:T(8,128)(2,1)} %fusion.20) | data formatting | bytes 1572864
  167.1 1.9 %reshape.245 = bf16[384,1024]{1,0:T(8,128)(2,1)} reshape(bf16[3,128,4,4,64]{4,3,2,1,0:T(4,128)(2,1)S(1)} %copy.56) | data formatting | bytes 1572864
  169.0 1.8 all-to-all-done.1
  170.8 1.3 gather_fusion.1
  172.2 1.1 fusion.49
  (52 shorter events, 2.3 us)
Async XLA Ops:
  7.2 78.6 %copy-start = (bf16[1,2048,128]{2,1,0:T(8,128)(2,1)S(1)}, bf16[1,2048,128]{2,1,0:T(8,128)(2,1)}, u32[]{:S(2)}) copy-start(bf16[1,2048,128]{2,1,0:T(8,128)(2,1)} %param.19) | copy-start | bytes 1572868
  7.2 78.5 %all-gather.3.cloned.1.call-start = ((), (), s32[]{:S(2)}) async-start(), calls=%async_computation.2 | async-start | bytes 4456448 | tf_op jit(solution)/shard_map/all_gather | solution.py:91
  17.8 73.1 %copy-start.7 = (bf16[1,2048,128]{2,1,0:T(8,128)(2,1)S(1)}, bf16[1,2048,128]{2,1,0:T(8,128)(2,1)}, u32[]{:S(2)}) copy-start(bf16[1,2048,128]{2,1,0:T(8,128)(2,1)} %param.20) | copy-start | bytes 1572868
  43.5 102.5 %all-gather.5.cloned.1.call-start = ((), (), s32[]{:S(2)}) async-start(), calls=%async_computation.3 | async-start | bytes 4456448 | tf_op jit(solution)/shard_map/all_gather | solution.py:98
  85.7 5.2 %copy-start.6 = (bf16[32,1,32,2048]{3,0,1,2:T(8,128)(2,1)S(1)}, bf16[32,1,32,2048]{3,0,1,2:T(8,128)(2,1)}, u32[]{:S(2)}) copy-start(bf16[32,1,32,2048]{3,0,1,2:T(8,128)(2,1)} %all-gather.3.cloned.1.call-done) | copy-start | bytes 12582916
  90.9 3.7 %copy-start.2 = (bf16[2,384,256]{2,1,0:T(8,128)(2,1)S(1)}, bf16[2,384,256]{2,1,0:T(8,128)(2,1)}, u32[]{:S(2)}) copy-start(bf16[2,384,256]{2,1,0:T(8,128)(2,1)} %param.12) | copy-start | bytes 1179652
  94.6 7.9 %copy-start.5 = (f32[16]{0:T(128)S(1)}, f32[16]{0:T(128)}, u32[]{:S(2)}) copy-start(f32[16]{0:T(128)} %param.13) | copy-start | bytes 196
  94.6 7.9 %copy-start.4 = (f32[256,2]{0,1:T(2,128)S(1)}, f32[256,2]{0,1:T(2,128)}, u32[]{:S(2)}) copy-start(f32[256,2]{0,1:T(2,128)} %param.18) | copy-start | bytes 6148
  94.6 8.0 %collective-permute-start = (bf16[2,128,256]{2,1,0:T(8,128)(2,1)S(1)}, bf16[2,128,256]{2,1,0:T(8,128)(2,1)S(1)}, u32[]{:S(2)}, u32[]{:S(2)}) collective-permute-start(bf16[2,128,256]{2,1,0:T(8,128)(2,1)S(1)} %slice.18), channel_id=1, source_target_pairs={{0,1},{1,2},{2,3},{3,4},{4,5},{5,6},{6,7},{7,8},{8,9},{9,10},{10,1... | collective-permute-start | bytes 393224 | tf_op jit(solution)/shard_map/ppermute | solution.py:17
  108.6 2.7 %copy-start.1 = (f32[3,4,256,128,4]{3,2,4,1,0:T(8,128)}, f32[3,4,256,128,4]{3,2,4,1,0:T(8,128)S(1)}, u32[]{:S(2)}) copy-start(f32[3,4,256,128,4]{3,2,4,1,0:T(8,128)S(1)} %get-tuple-element.9) | copy-start | bytes 18874372
  108.7 37.4 %copy-start.8 = (bf16[1,2048,128]{2,1,0:T(8,128)(2,1)S(1)}, bf16[1,2048,128]{2,1,0:T(8,128)(2,1)}, u32[]{:S(2)}) copy-start(bf16[1,2048,128]{2,1,0:T(8,128)(2,1)} %param.21) | copy-start | bytes 1572868
  112.9 46.2 %copy-start.3 = (bf16[2,3,128,4,64]{2,4,3,1,0:T(8,128)(2,1)S(1)}, bf16[2,3,128,4,64]{2,4,3,1,0:T(8,128)(2,1)}, u32[]{:S(2)}) copy-start(bf16[2,3,128,4,64]{2,4,3,1,0:T(8,128)(2,1)} %copy.32) | copy-start | bytes 1179652
  150.2 20.6 %all-to-all-start.1 = ((bf16[32,32,128]{2,1,0:T(8,128)(2,1)}), bf16[32,32,128]{2,1,0:T(8,128)(2,1)S(1)}, u32[]{:S(2)}, u32[]{:S(2)}) async-start(bf16[32,32,128]{2,1,0:T(8,128)(2,1)} %fusion.37), calls=%async_computation.1 | async-start | bytes 524288 | tf_op jit(solution)/shard_map/all_to_all | solution.py:103
Sparse Core Ops, SparseCore 0:
  43.7 42.0 all-gather.2
  94.7 51.2 all-gather.4
where the time goes:
time: 181 us; the launch traced here: 180 us
  waiting for transfers between devices  76.9 us (42%)
  blocking collectives  24.9 us (14%)
  local copies, waits for them, and re-layouts  21.3 us (12%)
  matrix products  20.4 us (11%)
  between operations  14.4 us (8%)
  starting transfers between devices  12.3 us (7%)
  other arithmetic  9.73 us (5%)
    all_gather x1, waiting for transfers between devices, route_experts(): block_rows = lax.all_gather(incoming, 'tp', axis=2, tiled=True)  42.1 us
    all_gather x1, waiting for transfers between devices, route_experts(): lax.all_gather(hidden, 'tp', axis=3, tiled=True)  33 us
    all_to_all x1, blocking collectives, route_experts(): lax.all_to_all(outgoing, 'ep', split_axis=0, concat_axis=0, tiled=True)  24.9 us
    all_to_all x1, starting transfers between devices, route_experts(): lax.all_to_all(produced, 'ep', split_axis=0, concat_axis=0, tiled=True)  8.95 us
    unnamed x21, local copies, waits for them, and re-layouts  7.39 us
    dot_general x1, matrix products, attend_window(): jnp.einsum('bhgqk,bkhd->bqhgd', weights.astype(jnp.bfloat16), banded[1],...  5.21 us
    dot_general x1, matrix products, route_experts(): jnp.einsum('secd,edf->secf', block_rows, w_gate, preferred_element_type=j...  5.18 us
    dot_general x1, matrix products, route_experts(): jnp.einsum('secf,efd->secd', lax.all_gather(hidden, 'tp', axis=3, tiled=T...  4.15 us
  transfers between devices with their start and end apart: 4, of which 3 were waited for; matrix products, arithmetic and copies ran while one was open for 12% of the time, Pallas kernels for 0%

commit v1 on v0

v1 whole, which is shorter than its diff:
```python
import functools

import jax
import jax.numpy as jnp
from jax import lax
from jax.experimental import pallas as pl
from jax.experimental.pallas import tpu as pltpu
from jax.sharding import PartitionSpec as P

QH = 16
KVH = 4
HD = 64
WINDOW = 128
EPG = 4
CAP = 32
HALF = CAP // 2
CW = 256
NSUB = 4

F32 = jnp.float32
BF16 = jnp.bfloat16


def iota(shape, dim):
    return lax.broadcasted_iota(jnp.int32, shape, dim)


def dot(a, b):
    return jnp.dot(a, b, preferred_element_type=F32)


def dot_t(a, b):
    return lax.dot_general(a, b, (((1,), (1,)), ((), ())), preferred_element_type=F32)


def kernel(
    n_ep,
    n_tp,
    q_hbm,
    kv_hbm,
    sink_ref,
    rows_hbm,
    gain_ref,
    chosen_ref,
    weight_ref,
    wg_hbm,
    wu_hbm,
    wd_hbm,
    att_hbm,
    mix_ref,
    rows_v,
    q_v,
    kv_v,
    wgu,
    wd,
    outb,
    xbuf,
    hbuf,
    acc,
    acc2,
    obuf,
    rbuf,
    att_v,
    pick,
    maskb,
    loc_sem,
    w_send,
    w_recv,
    edge_sem,
    d_send,
    d_recv,
    ring_send,
    ring_recv,
    r_send,
    r_recv,
):
    ep = lax.axis_index("ep")
    tp = lax.axis_index("tp")
    c = lax.rem(tp, 2)
    y = lax.div(tp, 2)
    ny = n_tp // 2
    steps = ny // 2
    slots = n_ep * HALF
    sr = slots // NSUB
    per_sub = n_ep // NSUB
    length = q_v.shape[0]
    blocks = length // WINDOW
    tokens = rows_v.shape[0]
    width = rows_v.shape[1]
    right = lax.rem(y + 1, ny)
    left = lax.rem(y + ny - 1, ny)

    def device(e, t):
        return {"ep": e, "tp": t}

    load_rows = pltpu.make_async_copy(rows_hbm, rows_v, loc_sem.at[0])
    load_q = pltpu.make_async_copy(q_hbm, q_v, loc_sem.at[1])
    load_kv = pltpu.make_async_copy(kv_hbm, kv_v.at[:, pl.ds(WINDOW, length), :], loc_sem.at[2])
    load_rows.start()
    load_q.start()
    load_kv.start()
    mine = pl.ds(pl.multiple_of(c * 128, 128), 128)
    mine_up = pl.ds(pl.multiple_of(c * 128 + CW, 128), 128)
    weight_ends = (
        (wg_hbm.at[0], wgu.at[:, mine]),
        (wu_hbm.at[0], wgu.at[:, mine_up]),
        (wd_hbm.at[0], wd.at[:, mine]),
    )
    load_w = [
        pltpu.make_async_copy(src, dst, loc_sem.at[3 + i]) for i, (src, dst) in enumerate(weight_ends)
    ]
    for copy in load_w:
        copy.start()

    barrier = pltpu.get_barrier_semaphore()
    plane = 2 * n_ep
    here = ep * 2 + c

    def greet(r, carry):
        other = lax.rem(here + r, plane)
        pl.semaphore_signal(
            barrier, inc=1, device_id=device(lax.div(other, 2), 2 * y + lax.rem(other, 2))
        )
        return carry

    lax.fori_loop(1, plane, greet, 0)
    pl.semaphore_signal(barrier, inc=1, device_id=device(ep, 2 * right + c))
    pl.semaphore_signal(barrier, inc=1, device_id=device(ep, 2 * left + c))
    flat = ep * n_tp + tp
    total = n_ep * n_tp
    after = lax.rem(flat + 1, total)
    before = lax.rem(flat + total - 1, total)
    after_dev = device(lax.div(after, n_tp), lax.rem(after, n_tp))
    pl.semaphore_signal(barrier, inc=1, device_id=after_dev)
    pl.semaphore_signal(
        barrier, inc=1, device_id=device(lax.div(before, n_tp), lax.rem(before, n_tp))
    )

    chosen = chosen_ref[...]
    lanes = iota((tokens, 128), 1)
    named = [chosen[:, k : k + 1] == lanes for k in range(2)]
    either = jnp.where(named[0] | named[1], 1.0, 0.0)
    lower = jnp.where(iota((tokens, tokens), 1) < iota((tokens, tokens), 0), 1.0, 0.0).astype(BF16)
    position = dot(lower, either.astype(BF16))
    spread = jnp.where(either > 0.5, position, -1.0).astype(BF16)
    repeat = jnp.where(
        lax.div(iota((slots, 128), 0), HALF) == iota((slots, 128), 1), 1.0, 0.0
    ).astype(BF16)
    wanted = (lax.rem(iota((slots, tokens), 0), HALF) + c * HALF).astype(F32)
    seats = jnp.where(dot_t(repeat, spread) == wanted, 1.0, 0.0).astype(BF16)

    load_rows.wait()
    square = jnp.zeros((tokens, 128), F32)
    for i in range(width // 128):
        part = rows_v[:, i * 128 : (i + 1) * 128].astype(F32)
        square = square + part * part
    mean = jnp.sum(square, axis=1, keepdims=True) * (1.0 / width)
    columns = pl.ds(pl.multiple_of(y * CW, CW), CW)
    normed = (
        rows_v[:, columns].astype(F32) * lax.rsqrt(mean + 1e-06) * gain_ref[:, columns]
    ).astype(BF16)
    outb[...] = dot(seats, normed).astype(BF16)

    pl.semaphore_wait(barrier, plane - 1 + 4)

    my_rows = pl.ds(pl.multiple_of(ep * HALF, HALF), HALF)
    my_sub = lax.div(ep, per_sub)

    def dispatch(r, carry):
        e = lax.rem(ep + r, n_ep)
        pltpu.make_async_remote_copy(
            src_ref=outb.at[pl.ds(pl.multiple_of(e * HALF, HALF), HALF)],
            dst_ref=xbuf.at[y, my_rows],
            send_sem=d_send.at[0],
            recv_sem=d_recv.at[my_sub],
            device_id=device(e, tp),
        ).start()
        return carry

    lax.fori_loop(1, n_ep, dispatch, 0)
    pltpu.make_async_copy(outb.at[my_rows], xbuf.at[y, my_rows], d_recv.at[my_sub]).start()

    edge = pltpu.make_async_remote_copy(
        src_ref=kv_hbm.at[:, pl.ds(length - WINDOW, WINDOW), :],
        dst_ref=kv_v.at[:, pl.ds(0, WINDOW), :],
        send_sem=edge_sem.at[0],
        recv_sem=edge_sem.at[1],
        device_id=after_dev,
    )
    edge.start()
    partner = device(ep, 2 * y + 1 - c)
    share_w = [
        pltpu.make_async_remote_copy(
            src_ref=src,
            dst_ref=dst,
            send_sem=w_send.at[i],
            recv_sem=w_recv.at[i],
            device_id=partner,
        )
        for i, (src, dst) in enumerate(weight_ends)
    ]
    for copy in share_w:
        copy.start()

    for k in range(2):
        seat = jnp.sum(jnp.where(named[k], position, 0.0), axis=1, keepdims=True)
        place = chosen[:, k : k + 1] * CAP + seat.astype(jnp.int32)
        pick[k] = jnp.where(place == iota((tokens, n_ep * CAP), 1), 1.0, 0.0).astype(BF16)

    gap = lax.rem(iota((2 * WINDOW, 2 * WINDOW), 0), WINDOW) + WINDOW - iota((2 * WINDOW, 2 * WINDOW), 1)
    maskb[...] = jnp.where((gap >= 0) & (gap < WINDOW), 0.0, -1e30)
    load_q.wait()
    load_kv.wait()

    def attend(b, p):
        rows = pl.ds(pl.multiple_of(b * WINDOW, WINDOW), WINDOW)
        key_rows = pl.ds(pl.multiple_of(b * WINDOW, WINDOW), 2 * WINDOW)
        pair = pl.ds(pl.multiple_of(p * 128, 128), 128)
        keys = kv_v[0, key_rows, pair]
        vals = kv_v[1, key_rows, pair]
        low_lane = iota((2 * WINDOW, 128), 1) < HD
        swap = jnp.where(
            lax.rem(iota((128, 128), 0) + HD, 128) == iota((128, 128), 1), 1.0, 0.0
        ).astype(BF16)
        zero = jnp.zeros((2 * WINDOW, 128), BF16)
        keys_sw = dot(keys, swap).astype(BF16)
        vals_sw = dot(vals, swap).astype(BF16)
        start = jnp.where((b == 0) & (flat == 0), -1e30, 0.0)
        visible = maskb[...] + jnp.where(iota((1, 2 * WINDOW), 1) < WINDOW, start, 0.0)
        for h in range(2):
            k_low, k_high = (keys, keys_sw) if h == 0 else (keys_sw, keys)
            v_low, v_high = (vals, vals_sw) if h == 0 else (vals_sw, vals)
            k_half = (jnp.where(low_lane, k_low, zero), jnp.where(low_lane, zero, k_high))
            v_half = (jnp.where(low_lane, v_low, zero), jnp.where(low_lane, zero, v_high))
            at = p * (8 * HD) + h * (4 * HD)
            tiles = [pl.ds(pl.multiple_of(at + i * 128, 128), 128) for i in range(2)]
            query = jnp.concatenate([q_v[rows, t] for t in tiles], axis=0)
            summed = None
            totals = []
            for i in range(2):
                scores = dot_t(query, k_half[i]) * (HD**-0.5) + visible
                head = p * 8 + h * 4 + i
                sink = jnp.where(
                    iota((2 * WINDOW, 1), 0) < WINDOW, sink_ref[head], sink_ref[head + 2]
                )
                highest = jnp.maximum(jnp.max(scores, axis=1, keepdims=True), sink)
                weights = jnp.exp(scores - highest)
                totals.append(jnp.sum(weights, axis=1, keepdims=True) + jnp.exp(sink - highest))
                part = dot(weights.astype(BF16), v_half[i])
                summed = part if summed is None else summed + part
            out = (summed / jnp.where(low_lane, totals[0], totals[1])).astype(BF16)
            for i in range(2):
                att_v[rows, tiles[i]] = out[i * WINDOW : (i + 1) * WINDOW]

    def attend_block(b):
        def body(p, carry):
            attend(b, p)
            return carry

        lax.fori_loop(0, 2, body, 0)

    def attend_tail(b, carry):
        attend_block(b)
        return carry

    lax.fori_loop(1, blocks, attend_tail, 0)

    def piece(buf, phase, way, t, sub, incoming):
        hop = t + 1 if incoming else t
        chunk = lax.rem(y + (ny - hop if way == 0 else hop), ny)
        part = buf.at[chunk, pl.ds(sub * sr, sr)]
        target = right if way == 0 else left
        return pltpu.make_async_remote_copy(
            src_ref=part,
            dst_ref=part,
            send_sem=ring_send.at[phase, way, t, sub],
            recv_sem=ring_recv.at[phase, way, t, sub],
            device_id=device(ep, 2 * target + c),
        )

    def travels(way, t, sub):
        return t < steps - 1 or (sub < NSUB // 2) == (way == 0)

    def add_chunk(buf, weights, total_ref, chunk, first):
        depth = weights[pl.ds(pl.multiple_of(chunk * CW, CW), CW), :]
        big = slots // 2

        def body(i, carry):
            rows = pl.ds(pl.multiple_of(i * big, big), big)
            value = dot(buf[chunk, rows], depth)
            if first:
                total_ref[rows, :] = value
            else:
                total_ref[rows, :] += value
            return carry

        lax.fori_loop(0, 2, body, 0)

    def ring(buf, weights, total_ref, phase, between):
        add_chunk(buf, weights, total_ref, y, True)
        for t in range(steps - 1):
            between(t)
            for sub in range(NSUB):
                for way in range(2):
                    piece(buf, phase, way, t, sub, True).wait_recv()
                    if travels(way, t + 1, sub):
                        piece(buf, phase, way, t + 1, sub, False).start()
            add_chunk(buf, weights, total_ref, lax.rem(y + ny - t - 1, ny), False)
            add_chunk(buf, weights, total_ref, lax.rem(y + t + 1, ny), False)

    def last_pieces(buf, phase, sub):
        way = 0 if sub < NSUB // 2 else 1
        piece(buf, phase, way, steps - 1, sub, True).wait_recv()

    far = lax.rem(y + steps, ny)
    far_rows = pl.ds(pl.multiple_of(far * CW, CW), CW)
    order = [sub for pair in zip(range(NSUB // 2), range(NSUB // 2, NSUB)) for sub in pair]

    for sub in range(NSUB):
        held = xbuf.at[y, pl.ds(sub * sr, sr)]
        pltpu.make_async_copy(held, held, d_recv.at[sub]).wait()
        for way in range(2):
            if travels(way, 0, sub):
                piece(xbuf, 0, way, 0, sub, False).start()
    for i in range(2):
        load_w[i].wait()
        share_w[i].wait_recv()

    def spare(t):
        if t == 0:
            edge.wait_recv()
            attend_block(0)
            pltpu.make_async_copy(att_v, att_hbm, loc_sem.at[6]).start()

    ring(xbuf, wgu, acc, 0, spare)
    for sub in order:
        rows = pl.ds(sub * sr, sr)
        last_pieces(xbuf, 0, sub)
        both = acc[rows, :] + dot(xbuf[far, rows], wgu[far_rows, :])
        gate = both[:, :CW]
        hbuf[y, rows] = (gate / (1.0 + jnp.exp(-gate)) * both[:, CW:]).astype(BF16)
        for way in range(2):
            if travels(way, 0, sub):
                piece(hbuf, 1, way, 0, sub, False).start()
    load_w[2].wait()
    share_w[2].wait_recv()
    ring(hbuf, wd, acc2, 1, lambda t: None)

    back_rows = pl.ds(pl.multiple_of(ep * CAP + c * HALF, HALF), HALF)
    for sub in order:
        rows = pl.ds(sub * sr, sr)
        last_pieces(hbuf, 1, sub)
        obuf[rows, :] = (acc2[rows, :] + dot(hbuf[far, rows], wd[far_rows, :])).astype(BF16)

        def give_back(i, carry):
            s = sub * per_sub + i
            from_rows = pl.ds(pl.multiple_of(s * HALF, HALF), HALF)
            theirs = pl.ds(pl.multiple_of((1 - c) * 128, 128), 128)
            pltpu.make_async_remote_copy(
                src_ref=obuf.at[from_rows, theirs],
                dst_ref=rbuf.at[back_rows],
                send_sem=r_send.at[0],
                recv_sem=r_recv.at[0],
                device_id=device(s, 2 * y + 1 - c),
            ).start()

            @pl.when(s != ep)
            def _():
                pltpu.make_async_remote_copy(
                    src_ref=obuf.at[from_rows, mine],
                    dst_ref=rbuf.at[back_rows],
                    send_sem=r_send.at[1],
                    recv_sem=r_recv.at[0],
                    device_id=device(s, tp),
                ).start()

            @pl.when(s == ep)
            def _():
                pltpu.make_async_copy(
                    obuf.at[from_rows, mine], rbuf.at[back_rows], r_recv.at[0]
                ).start()

            return carry

        lax.fori_loop(0, per_sub, give_back, 0)

    for phase, buf in ((0, xbuf), (1, hbuf)):
        for way in range(2):
            for t in range(steps):
                for sub in range(NSUB):
                    if travels(way, t, sub):
                        piece(buf, phase, way, t, sub, False).wait_send()
    sent = outb.at[pl.ds(0, slots - HALF)]
    pltpu.make_async_copy(sent, sent, d_send.at[0]).wait()
    edge.wait_send()
    for copy in share_w:
        copy.wait_send()
    pltpu.make_async_copy(att_v, att_hbm, loc_sem.at[6]).wait()

    pltpu.make_async_copy(rbuf, rbuf, r_recv.at[0]).wait()
    mixed = weight_ref[:, 0:1] * dot(pick[0], rbuf[...])
    mixed = mixed + weight_ref[:, 1:2] * dot(pick[1], rbuf[...])
    mix_ref[...] = mixed.astype(BF16)

    back = obuf.at[:, pl.ds(0, 128)]
    pltpu.make_async_copy(back, back, r_send.at[0]).wait()
    back_less = obuf.at[pl.ds(0, slots - HALF), pl.ds(0, 128)]
    pltpu.make_async_copy(back_less, back_less, r_send.at[1]).wait()


def shards(
    n_ep,
    n_tp,
    queries,
    keys_values,
    sink_logits,
    moe_rows,
    norm_gain,
    group_choice,
    member_choice,
    route_weight,
    w_gate,
    w_up,
    w_down,
):
    tokens, width = moe_rows.shape
    length = queries.shape[0]
    slots = n_ep * HALF
    ny = n_tp // 2
    steps = ny // 2
    chosen = group_choice[:, None] * EPG + member_choice
    hbm = pl.BlockSpec(memory_space=pl.ANY)
    vmem = pl.BlockSpec(memory_space=pltpu.VMEM)
    smem = pl.BlockSpec(memory_space=pltpu.SMEM)
    dma = pltpu.SemaphoreType.DMA
    return pl.pallas_call(
        functools.partial(kernel, n_ep, n_tp),
        out_shape=(
            jax.ShapeDtypeStruct(queries.shape, BF16),
            jax.ShapeDtypeStruct((tokens, 128), BF16),
        ),
        in_specs=[hbm, hbm, smem, hbm, vmem, vmem, vmem, hbm, hbm, hbm],
        out_specs=(hbm, vmem),
        scratch_shapes=[
            pltpu.VMEM((tokens, width), BF16),
            pltpu.VMEM((length, QH * HD), BF16),
            pltpu.VMEM((2, length + WINDOW, KVH * HD), BF16),
            pltpu.VMEM((width, 2 * CW), BF16),
            pltpu.VMEM((width, CW), BF16),
            pltpu.VMEM((slots, CW), BF16),
            pltpu.VMEM((ny, slots, CW), BF16),
            pltpu.VMEM((ny, slots, CW), BF16),
            pltpu.VMEM((slots, 2 * CW), F32),
            pltpu.VMEM((slots, CW), F32),
            pltpu.VMEM((slots, CW), BF16),
            pltpu.VMEM((n_ep * CAP, 128), BF16),
            pltpu.VMEM((length, QH * HD), BF16),
            pltpu.VMEM((2, tokens, n_ep * CAP), BF16),
            pltpu.VMEM((2 * WINDOW, 2 * WINDOW), F32),
            dma((7,)),
            dma((3,)),
            dma((3,)),
            dma((2,)),
            dma((1,)),
            dma((NSUB,)),
            dma((2, 2, steps, NSUB)),
            dma((2, 2, steps, NSUB)),
            dma((2,)),
            dma((1,)),
        ],
        compiler_params=pltpu.CompilerParams(
            collective_id=0, has_side_effects=True, vmem_limit_bytes=50 * 2**20
        ),
        name="step",
    )(
        queries,
        keys_values,
        sink_logits,
        moe_rows,
        norm_gain.reshape(1, width),
        chosen,
        route_weight,
        w_gate,
        w_up,
        w_down,
    )


def solution(mesh):
    in_specs = (
        P(("ep", "tp"), None),
        P(None, ("ep", "tp"), None),
        P(),
        P("ep", None),
        P(),
        P("ep"),
        P("ep", None),
        P("ep", None),
        P("ep", None, "tp"),
        P("ep", None, "tp"),
        P("ep", None, "tp"),
    )
    out_specs = (P(("ep", "tp"), None), P("ep", "tp"))
    body = functools.partial(shards, mesh.shape["ep"], mesh.shape["tp"])
    return jax.shard_map(body, mesh=mesh, in_specs=in_specs, out_specs=out_specs, check_vma=False)
```

time: 181 us -> 84.3 us (0.47)
  waiting for transfers between devices: 76.9 us -> 0 us
  Pallas kernels: 0 us -> 75 us
  blocking collectives: 24.9 us -> 0 us
  matrix products: 20.4 us -> 0 us
  local copies, waits for them, and re-layouts: 21.3 us -> 7.36 us
  between operations: 14.4 us -> 0.72 us
  starting transfers between devices: 12.3 us -> 0 us
  other arithmetic: 9.73 us -> 0.84 us
    all_gather x2 -> x0, waiting for transfers between devices: 75.1 us -> none  [the longest x1 42.1 us: route_experts(): block_rows = lax.all_gather(incoming, 'tp', axis=2, tiled=True)]
    pallas_call x0 -> x1, Pallas kernels: none -> 75 us  [shards(): pl.pallas_call(functools.partial(kernel, n_ep, n_tp), out_shape=(jax.Shap...]
    all_to_all x1 -> x0, blocking collectives: 24.9 us -> none  [route_experts(): lax.all_to_all(outgoing, 'ep', split_axis=0, concat_axis=0, tiled=True)]
    dot_general x5 -> x0, matrix products: 20.4 us -> none  [the longest x1 5.21 us: attend_window(): jnp.einsum('bhgqk,bkhd->bqhgd', weights.astype(jnp.bfloat16), banded[1],...]
    all_to_all x1 -> x0, starting transfers between devices: 8.95 us -> none  [route_experts(): lax.all_to_all(produced, 'ep', split_axis=0, concat_axis=0, tiled=True)]
    reshape x8 -> x0, local copies, waits for them, and re-layouts: 7.42 us -> none  [the longest x1 3.37 us: attend_window(): query_blocks = queries.reshape(blocks, WINDOW, KVH, sharing, HD)]
    reduce_sum x4 -> x0, other arithmetic: 4.3 us -> none  [the longest x1 1.63 us: attend_window(): totals = jnp.sum(weights, axis=-1) + jnp.exp(sink_column - highest)]
    ppermute x1 -> x0, starting transfers between devices: 3.29 us -> none  [passed_along(): return lax.ppermute(value, axis, pairs)]
  transfers between devices with their start and end apart: 4 -> 0, of which waited for: 3 -> 0; matrix products, arithmetic and copies ran while one was open for 12% -> 0% of each run, Pallas kernels for 0% -> 0%
where the time goes in v1:
time: 84.3 us; the launch traced here: 83.9 us
  Pallas kernels  75 us (89%)
  local copies, waits for them, and re-layouts  7.36 us (9%)
    pallas_call x1, Pallas kernels, shards(): pl.pallas_call(functools.partial(kernel, n_ep, n_tp), out_shape=(jax.Shap...  75 us
    unnamed x18, local copies, waits for them, and re-layouts  7.36 us

profile of v1, /device:TPU:1, one launch (start us, length us, event | category | flops | bytes accessed | tf_op | source)
XLA Modules:
  0.0 83.9 jit_solution(12251704478925050209)
XLA Ops:
  0.6 0.0 copy-start.1
  0.6 0.7 broadcast_multiply_fusion
  1.4 0.8 copy.16
  2.2 0.1 broadcast_add_fusion.chosen_ref
  2.3 0.0 copy-start.5
  2.3 0.0 copy-start.6
  2.3 0.8 copy.17.weight_ref
  3.2 0.0 copy-done.1
  3.2 0.0 copy-done.5
  3.2 0.0 copy-done.6
  3.2 0.0 copy-start
  3.2 1.1 %copy-done = bf16[384,1024]{1,0:T(8,128)(2,1)S(1)} copy-done((bf16[384,1024]{1,0:T(8,128)(2,1)S(1)}, bf16[384,1024]{1,0:T(8,128)(2,1)}, u32[]{:S(2)}) %copy-start) | copy-done | bytes 786456
  4.3 0.0 copy-start.2
  4.3 1.0 %copy-done.2 = bf16[1,2048,128]{2,1,0:T(8,128)(2,1)S(1)} copy-done((bf16[1,2048,128]{2,1,0:T(8,128)(2,1)S(1)}, bf16[1,2048,128]{2,1,0:T(8,128)(2,1)}, u32[]{:S(2)}) %copy-start.2) | copy-done | bytes 524312
  5.4 0.0 copy-start.3
  5.4 1.0 %copy-done.3 = bf16[1,2048,128]{2,1,0:T(8,128)(2,1)S(1)} copy-done((bf16[1,2048,128]{2,1,0:T(8,128)(2,1)S(1)}, bf16[1,2048,128]{2,1,0:T(8,128)(2,1)}, u32[]{:S(2)}) %copy-start.3) | copy-done | bytes 524312
  6.4 0.0 copy-start.4
  6.4 1.0 %copy-done.4 = bf16[2,384,256]{2,1,0:T(8,128)(2,1)S(1)} copy-done((bf16[2,384,256]{2,1,0:T(8,128)(2,1)S(1)}, bf16[2,384,256]{2,1,0:T(8,128)(2,1)}, u32[]{:S(2)}) %copy-start.4) | copy-done | bytes 393240
  7.4 75.0 %step.1 = (bf16[384,1024]{1,0:T(8,128)(2,1)S(1)}, bf16[256,128]{1,0:T(8,128)(2,1)S(1)}) custom-call(bf16[384,1024]{1,0:T(8,128)(2,1)S(1)} %copy-done, bf16[2,384,256]{2,1,0:T(8,128)(2,1)S(1)} %copy-done.4, f32[16]{0:T(128)S(1)} %copy-done.6, bf16[256,2048]{1,0:T(8,128)(2,1)} %rows_hbm.1, f32[1,2048]{1,0:T(1,128)S(1)} %bitcast.1, ...), custom_call_target="tpu_custom_call" | custom-call | tf_op jit(solution)/shard_map/step/pallas_call | solution.py:436
  82.4 0.9 %copy.20 = bf16[384,1024]{1,0:T(8,128)(2,1)} copy(bf16[384,1024]{1,0:T(8,128)(2,1)S(1)} %get-tuple-element.4) | data formatting | bytes 1572864
  83.3 0.6 copy.21
Async XLA Ops:
  0.6 2.5 %copy-start.1 = (bf16[1,2048,128]{2,1,0:T(8,128)(2,1)S(1)}, bf16[1,2048,128]{2,1,0:T(8,128)(2,1)}, u32[]{:S(2)}) copy-start(bf16[1,2048,128]{2,1,0:T(8,128)(2,1)} %wg_hbm.1) | copy-start | bytes 1572868
  2.3 0.9 %copy-start.5 = (f32[2048]{0:T(1024)S(1)}, f32[2048]{0:T(1024)}, u32[]{:S(2)}) copy-start(f32[2048]{0:T(1024)} %param.15) | copy-start | bytes 24580
  2.3 0.9 %copy-start.6 = (f32[16]{0:T(128)S(1)}, f32[16]{0:T(128)}, u32[]{:S(2)}) copy-start(f32[16]{0:T(128)} %sink_ref.1) | copy-start | bytes 196
  3.2 1.1 %copy-start = (bf16[384,1024]{1,0:T(8,128)(2,1)S(1)}, bf16[384,1024]{1,0:T(8,128)(2,1)}, u32[]{:S(2)}) copy-start(bf16[384,1024]{1,0:T(8,128)(2,1)} %q_hbm.1) | copy-start | bytes 2359300
  4.3 1.0 %copy-start.2 = (bf16[1,2048,128]{2,1,0:T(8,128)(2,1)S(1)}, bf16[1,2048,128]{2,1,0:T(8,128)(2,1)}, u32[]{:S(2)}) copy-start(bf16[1,2048,128]{2,1,0:T(8,128)(2,1)} %wu_hbm.1) | copy-start | bytes 1572868
  5.4 1.0 %copy-start.3 = (bf16[1,2048,128]{2,1,0:T(8,128)(2,1)S(1)}, bf16[1,2048,128]{2,1,0:T(8,128)(2,1)}, u32[]{:S(2)}) copy-start(bf16[1,2048,128]{2,1,0:T(8,128)(2,1)} %wd_hbm.1) | copy-start | bytes 1572868
  6.4 1.0 %copy-start.4 = (bf16[2,384,256]{2,1,0:T(8,128)(2,1)S(1)}, bf16[2,384,256]{2,1,0:T(8,128)(2,1)}, u32[]{:S(2)}) copy-start(bf16[2,384,256]{2,1,0:T(8,128)(2,1)} %kv_hbm.1) | copy-start | bytes 1179652

commit v2 on v1

v2 whole, which is shorter than its diff:
```python
import functools

import jax
import jax.numpy as jnp
from jax import lax
from jax.experimental import pallas as pl
from jax.experimental.pallas import tpu as pltpu
from jax.sharding import PartitionSpec as P

QH = 16
KVH = 4
HD = 64
WINDOW = 128
EPG = 4
CAP = 32
HALF = CAP // 2
CW = 256
NSUB = 4

F32 = jnp.float32
BF16 = jnp.bfloat16


def iota(shape, dim):
    return lax.broadcasted_iota(jnp.int32, shape, dim)


def dot(a, b):
    return jnp.dot(a, b, preferred_element_type=F32)


def dot_t(a, b):
    return lax.dot_general(a, b, (((1,), (1,)), ((), ())), preferred_element_type=F32)


def kernel(
    n_ep,
    n_tp,
    q_hbm,
    kv_hbm,
    sink_hbm,
    rows_hbm,
    gain_hbm,
    group_hbm,
    member_hbm,
    weight_hbm,
    wg_hbm,
    wu_hbm,
    wd_hbm,
    att_out,
    mix_ref,
    sink_ref,
    gain_ref,
    group_ref,
    member_ref,
    weight_ref,
    rows_v,
    q_v,
    kv_v,
    wgu,
    wd,
    outb,
    xbuf,
    hbuf,
    acc,
    acc2,
    obuf,
    rbuf,
    att_v,
    pick,
    maskb,
    share,
    loc_sem,
    w_send,
    w_recv,
    edge_sem,
    d_send,
    d_recv,
    ring_send,
    ring_recv,
    r_send,
    r_recv,
):
    ep = lax.axis_index("ep")
    tp = lax.axis_index("tp")
    c = lax.rem(tp, 2)
    y = lax.div(tp, 2)
    ny = n_tp // 2
    steps = ny // 2
    slots = n_ep * HALF
    sr = slots // NSUB
    per_sub = n_ep // NSUB
    length = q_v.shape[0]
    blocks = length // WINDOW
    tokens = rows_v.shape[0]
    width = rows_v.shape[1]
    right = lax.rem(y + 1, ny)
    left = lax.rem(y + ny - 1, ny)

    def device(e, t):
        return {"ep": e, "tp": t}

    load_rows = pltpu.make_async_copy(rows_hbm, rows_v, loc_sem.at[0])
    load_q = pltpu.make_async_copy(q_hbm, q_v, loc_sem.at[1])
    load_kv = pltpu.make_async_copy(kv_hbm, kv_v.at[:, pl.ds(WINDOW, length), :], loc_sem.at[2])
    small = [
        pltpu.make_async_copy(src, dst, loc_sem.at[7 + i])
        for i, (src, dst) in enumerate(
            (
                (group_hbm, group_ref),
                (member_hbm, member_ref),
                (gain_hbm, gain_ref),
                (weight_hbm, weight_ref),
                (sink_hbm, sink_ref),
            )
        )
    ]
    for copy in small:
        copy.start()
    load_rows.start()
    load_q.start()
    load_kv.start()
    mine = pl.ds(pl.multiple_of(c * 128, 128), 128)
    mine_up = pl.ds(pl.multiple_of(c * 128 + CW, 128), 128)
    weight_ends = (
        (wg_hbm.at[0], wgu.at[:, mine]),
        (wu_hbm.at[0], wgu.at[:, mine_up]),
        (wd_hbm.at[0], wd.at[:, mine]),
    )
    load_w = [
        pltpu.make_async_copy(src, dst, loc_sem.at[3 + i]) for i, (src, dst) in enumerate(weight_ends)
    ]
    for copy in load_w:
        copy.start()

    barrier = pltpu.get_barrier_semaphore()
    plane = 2 * n_ep
    here = ep * 2 + c

    def greet(r, carry):
        other = lax.rem(here + r, plane)
        pl.semaphore_signal(
            barrier, inc=1, device_id=device(lax.div(other, 2), 2 * y + lax.rem(other, 2))
        )
        return carry

    with jax.named_scope("greet"):
        lax.fori_loop(1, plane, greet, 0)
    pl.semaphore_signal(barrier, inc=1, device_id=device(ep, 2 * right + c))
    pl.semaphore_signal(barrier, inc=1, device_id=device(ep, 2 * left + c))
    flat = ep * n_tp + tp
    total = n_ep * n_tp
    after = lax.rem(flat + 1, total)
    before = lax.rem(flat + total - 1, total)
    after_dev = device(lax.div(after, n_tp), lax.rem(after, n_tp))
    pl.semaphore_signal(barrier, inc=1, device_id=after_dev)
    pl.semaphore_signal(
        barrier, inc=1, device_id=device(lax.div(before, n_tp), lax.rem(before, n_tp))
    )

    with jax.named_scope("routing"):
        small[0].wait()
        small[1].wait()
        chosen = group_ref[...] * EPG + member_ref[...]
        experts = iota((128, tokens), 0)
        named = [chosen[k : k + 1, :] == experts for k in range(2)]
        either = named[0] | named[1]
        upper = jnp.where(
            iota((tokens, tokens), 0) < iota((tokens, tokens), 1), 1.0, 0.0
        ).astype(BF16)
        position = dot(jnp.where(either, 1.0, 0.0).astype(BF16), upper)
        spread = jnp.where(either, position, -1.0).astype(BF16)
        repeat = jnp.where(
            lax.div(iota((slots, 128), 0), HALF) == iota((slots, 128), 1), 1.0, 0.0
        ).astype(BF16)
        wanted = (lax.rem(iota((slots, tokens), 0), HALF) + c * HALF).astype(F32)
        seats = jnp.where(dot(repeat, spread) == wanted, 1.0, 0.0).astype(BF16)

    with jax.named_scope("norm"):
        load_rows.wait()
        small[2].wait()
        square = jnp.zeros((tokens, 128), F32)
        for i in range(width // 128):
            part = rows_v[:, i * 128 : (i + 1) * 128].astype(F32)
            square = square + part * part
        mean = jnp.sum(square, axis=1, keepdims=True) * (1.0 / width)
        columns = pl.ds(pl.multiple_of(y * CW, CW), CW)
        normed = (
            rows_v[:, columns].astype(F32) * lax.rsqrt(mean + 1e-06) * gain_ref[:, columns]
        ).astype(BF16)
        outb[...] = dot(seats, normed).astype(BF16)

    with jax.named_scope("barrier"):
        pl.semaphore_wait(barrier, plane - 1 + 4)

    def offset(j):
        return jnp.where(lax.rem(j, 2) == 1, lax.div(j + 1, 2), lax.rem(n_ep - lax.div(j, 2), n_ep))

    def block(j):
        return pl.ds(pl.multiple_of(j * HALF, HALF), HALF)

    def dispatch(j, carry):
        e = lax.rem(ep + offset(j), n_ep)
        pltpu.make_async_remote_copy(
            src_ref=outb.at[block(e)],
            dst_ref=xbuf.at[y, block(j)],
            send_sem=d_send.at[0],
            recv_sem=d_recv.at[lax.div(j, per_sub)],
            device_id=device(e, tp),
        ).start()
        return carry

    with jax.named_scope("dispatch"):
        lax.fori_loop(1, n_ep, dispatch, 0)
        pltpu.make_async_copy(outb.at[block(ep)], xbuf.at[y, block(0)], d_recv.at[0]).start()

    edge = pltpu.make_async_remote_copy(
        src_ref=kv_hbm.at[:, pl.ds(length - WINDOW, WINDOW), :],
        dst_ref=kv_v.at[:, pl.ds(0, WINDOW), :],
        send_sem=edge_sem.at[0],
        recv_sem=edge_sem.at[1],
        device_id=after_dev,
    )
    edge.start()
    partner = device(ep, 2 * y + 1 - c)
    share_w = [
        pltpu.make_async_remote_copy(
            src_ref=src,
            dst_ref=dst,
            send_sem=w_send.at[i],
            recv_sem=w_recv.at[i],
            device_id=partner,
        )
        for i, (src, dst) in enumerate(weight_ends)
    ]
    with jax.named_scope("shares"):
        for copy in share_w:
            copy.start()

    with jax.named_scope("pick"):
        small[3].wait()
        sheet = [weight_ref[...]]
        for k in range(2):
            seat = jnp.sum(jnp.where(named[k], position, 0.0), axis=0, keepdims=True)
            sheet.append(chosen[k : k + 1, :].astype(F32) * CAP + seat)
        sheet.append(jnp.zeros((4, tokens), F32))
        upright = jnp.concatenate(sheet, axis=0).T
        share[...] = upright
        for k in range(2):
            place = upright[:, 2 + k : 3 + k].astype(jnp.int32)
            pick[k] = jnp.where(place == iota((tokens, n_ep * CAP), 1), 1.0, 0.0).astype(BF16)

    gap = lax.rem(iota((2 * WINDOW, 2 * WINDOW), 0), WINDOW) + WINDOW - iota((2 * WINDOW, 2 * WINDOW), 1)
    maskb[...] = jnp.where((gap >= 0) & (gap < WINDOW), 0.0, -1e30)
    with jax.named_scope("loads"):
        load_q.wait()
        load_kv.wait()
        small[4].wait()

    def attend(b, p):
        rows = pl.ds(pl.multiple_of(b * WINDOW, WINDOW), WINDOW)
        key_rows = pl.ds(pl.multiple_of(b * WINDOW, WINDOW), 2 * WINDOW)
        pair = pl.ds(pl.multiple_of(p * 128, 128), 128)
        keys = kv_v[0, key_rows, pair]
        vals = kv_v[1, key_rows, pair]
        low_lane = iota((2 * WINDOW, 128), 1) < HD
        swap = jnp.where(
            lax.rem(iota((128, 128), 0) + HD, 128) == iota((128, 128), 1), 1.0, 0.0
        ).astype(BF16)
        zero = jnp.zeros((2 * WINDOW, 128), BF16)
        keys_sw = dot(keys, swap).astype(BF16)
        vals_sw = dot(vals, swap).astype(BF16)
        start = jnp.where((b == 0) & (flat == 0), -1e30, 0.0)
        visible = maskb[...] + jnp.where(iota((1, 2 * WINDOW), 1) < WINDOW, start, 0.0)
        for h in range(2):
            k_low, k_high = (keys, keys_sw) if h == 0 else (keys_sw, keys)
            v_low, v_high = (vals, vals_sw) if h == 0 else (vals_sw, vals)
            k_half = (jnp.where(low_lane, k_low, zero), jnp.where(low_lane, zero, k_high))
            v_half = (jnp.where(low_lane, v_low, zero), jnp.where(low_lane, zero, v_high))
            at = p * (8 * HD) + h * (4 * HD)
            tiles = [pl.ds(pl.multiple_of(at + i * 128, 128), 128) for i in range(2)]
            query = jnp.concatenate([q_v[rows, t] for t in tiles], axis=0)
            summed = None
            totals = []
            for i in range(2):
                scores = dot_t(query, k_half[i]) * (HD**-0.5) + visible
                head = p * 8 + h * 4 + i
                sink = jnp.where(
                    iota((2 * WINDOW, 1), 0) < WINDOW, sink_ref[head], sink_ref[head + 2]
                )
                highest = jnp.maximum(jnp.max(scores, axis=1, keepdims=True), sink)
                weights = jnp.exp(scores - highest)
                totals.append(jnp.sum(weights, axis=1, keepdims=True) + jnp.exp(sink - highest))
                part = dot(weights.astype(BF16), v_half[i])
                summed = part if summed is None else summed + part
            out = (summed / jnp.where(low_lane, totals[0], totals[1])).astype(BF16)
            for i in range(2):
                att_v[rows, tiles[i]] = out[i * WINDOW : (i + 1) * WINDOW]

    def attend_tail(i, carry):
        attend(1 + lax.div(i, 2), lax.rem(i, 2))
        return carry

    with jax.named_scope("attend"):
        lax.fori_loop(0, 2 * (blocks - 1), attend_tail, 0)

    def piece(buf, phase, way, t, sub, incoming):
        hop = t + 1 if incoming else t
        chunk = lax.rem(y + (ny - hop if way == 0 else hop), ny)
        part = buf.at[chunk, pl.ds(sub * sr, sr)]
        target = right if way == 0 else left
        return pltpu.make_async_remote_copy(
            src_ref=part,
            dst_ref=part,
            send_sem=ring_send.at[phase, way, t, sub],
            recv_sem=ring_recv.at[phase, way, t, sub],
            device_id=device(ep, 2 * target + c),
        )

    def travels(way, t, sub):
        return t < steps - 1 or (sub % 2 == 0) == (way == 0)

    def send(buf, phase, t, sub):
        for way in range(2):
            if travels(way, t, sub):
                piece(buf, phase, way, t, sub, False).start()

    def add_chunk(buf, weights, total_ref, chunk, first=False):
        value = dot(buf[chunk], weights[pl.ds(pl.multiple_of(chunk * CW, CW), CW), :])
        if first:
            total_ref[...] = value
        else:
            total_ref[...] += value

    def ring(buf, weights, total_ref, phase, between):
        add_chunk(buf, weights, total_ref, y, True)
        for t in range(steps - 1):
            for sub in range(NSUB):
                for way in range(2):
                    piece(buf, phase, way, t, sub, True).wait_recv()
                    if travels(way, t + 1, sub):
                        piece(buf, phase, way, t + 1, sub, False).start()
            between(t)
            add_chunk(buf, weights, total_ref, lax.rem(y + ny - t - 1, ny))
            add_chunk(buf, weights, total_ref, lax.rem(y + t + 1, ny))

    def last_piece(buf, phase, sub):
        way = 0 if travels(0, steps - 1, sub) else 1
        piece(buf, phase, way, steps - 1, sub, True).wait_recv()

    far = lax.rem(y + steps, ny)
    far_rows = pl.ds(pl.multiple_of(far * CW, CW), CW)

    def hide(sub):
        last_piece(xbuf, 0, sub)
        rows = pl.ds(sub * sr, sr)
        both = acc[rows, :] + dot(xbuf[far, rows], wgu[far_rows, :])
        gate = both[:, :CW]
        hbuf[y, rows] = (gate / (1.0 + jnp.exp(-gate)) * both[:, CW:]).astype(BF16)
        send(hbuf, 1, 0, sub)

    def give_back(j, carry):
        s = lax.rem(ep + n_ep - offset(j), n_ep)
        theirs = pl.ds(pl.multiple_of((1 - c) * 128, 128), 128)
        pltpu.make_async_remote_copy(
            src_ref=obuf.at[block(j), theirs],
            dst_ref=rbuf.at[back_rows],
            send_sem=r_send.at[0],
            recv_sem=r_recv.at[0],
            device_id=device(s, 2 * y + 1 - c),
        ).start()

        @pl.when(s != ep)
        def _():
            pltpu.make_async_remote_copy(
                src_ref=obuf.at[block(j), mine],
                dst_ref=rbuf.at[back_rows],
                send_sem=r_send.at[1],
                recv_sem=r_recv.at[0],
                device_id=device(s, tp),
            ).start()

        @pl.when(s == ep)
        def _():
            pltpu.make_async_copy(
                obuf.at[block(j), mine], rbuf.at[back_rows], r_recv.at[0]
            ).start()

        return carry

    back_rows = pl.ds(pl.multiple_of(ep * CAP + c * HALF, HALF), HALF)

    def finish(sub):
        last_piece(hbuf, 1, sub)
        rows = pl.ds(sub * sr, sr)
        obuf[rows, :] = (acc2[rows, :] + dot(hbuf[far, rows], wd[far_rows, :])).astype(BF16)
        lax.fori_loop(sub * per_sub, (sub + 1) * per_sub, give_back, 0)

    def arrive(sub):
        held = xbuf.at[y, pl.ds(sub * sr, sr)]
        pltpu.make_async_copy(held, held, d_recv.at[sub]).wait()
        send(xbuf, 0, 0, sub)

    def early(t):
        if t == 0:
            edge.wait_recv()
        for p in range(2):
            if t == min(p, steps - 2):
                attend(0, p)
        if t == steps - 2:
            pltpu.make_async_copy(att_v, att_out, loc_sem.at[6]).start()

    with jax.named_scope("arrive"):
        for sub in range(NSUB):
            arrive(sub)
    with jax.named_scope("weights"):
        for i in range(2):
            load_w[i].wait()
            share_w[i].wait_recv()
    with jax.named_scope("ringx"):
        ring(xbuf, wgu, acc, 0, early)
    with jax.named_scope("middle"):
        for sub in range(NSUB):
            hide(sub)
    load_w[2].wait()
    share_w[2].wait_recv()
    with jax.named_scope("ringh"):
        ring(hbuf, wd, acc2, 1, lambda t: None)
    with jax.named_scope("down"):
        for sub in range(NSUB):
            finish(sub)

    with jax.named_scope("close"):
        for phase, buf in ((0, xbuf), (1, hbuf)):
            for way in range(2):
                for t in range(steps):
                    for sub in range(NSUB):
                        if travels(way, t, sub):
                            piece(buf, phase, way, t, sub, False).wait_send()
        sent = outb.at[pl.ds(0, slots - HALF)]
        pltpu.make_async_copy(sent, sent, d_send.at[0]).wait()
        edge.wait_send()
        for copy in share_w:
            copy.wait_send()
        pltpu.make_async_copy(att_v, att_out, loc_sem.at[6]).wait()

    with jax.named_scope("home"):
        pltpu.make_async_copy(rbuf, rbuf, r_recv.at[0]).wait()
    with jax.named_scope("mix"):
        mixed = share[:, 0:1] * dot(pick[0], rbuf[...])
        mixed = mixed + share[:, 1:2] * dot(pick[1], rbuf[...])
        mix_ref[...] = mixed.astype(BF16)

    back = obuf.at[:, pl.ds(0, 128)]
    pltpu.make_async_copy(back, back, r_send.at[0]).wait()
    back_less = obuf.at[pl.ds(0, slots - HALF), pl.ds(0, 128)]
    pltpu.make_async_copy(back_less, back_less, r_send.at[1]).wait()


def hand_on(att_in, mix_in, att_out, mix_out, att_v, mix_v, sem):
    pieces = 4
    size = att_v.shape[0] // pieces
    ways = [(mix_in, mix_v, mix_out)]
    for i in range(pieces):
        part = pl.ds(i * size, size)
        ways.append((att_in.at[part], att_v.at[part], att_out.at[part]))
    loads = [pltpu.make_async_copy(a, b, sem.at[0, i]) for i, (a, b, _) in enumerate(ways)]
    stores = [pltpu.make_async_copy(b, c, sem.at[1, i]) for i, (_, b, c) in enumerate(ways)]
    for load in loads:
        load.start()
    for load, store in zip(loads, stores):
        load.wait()
        store.start()
    for store in stores:
        store.wait()


def shards(
    n_ep,
    n_tp,
    queries,
    keys_values,
    sink_logits,
    moe_rows,
    norm_gain,
    group_choice,
    member_choice,
    route_weight,
    w_gate,
    w_up,
    w_down,
):
    tokens, width = moe_rows.shape
    length = queries.shape[0]
    slots = n_ep * HALF
    ny = n_tp // 2
    steps = ny // 2
    hbm = pl.BlockSpec(memory_space=pl.ANY)
    vmem = pl.BlockSpec(memory_space=pltpu.VMEM)
    dma = pltpu.SemaphoreType.DMA
    attended, mixed = pl.pallas_call(
        functools.partial(kernel, n_ep, n_tp),
        out_shape=(
            jax.ShapeDtypeStruct(queries.shape, BF16),
            jax.ShapeDtypeStruct((tokens, 128), BF16),
        ),
        in_specs=[hbm] * 11,
        out_specs=(hbm, vmem),
        scratch_shapes=[
            pltpu.SMEM((QH,), F32),
            pltpu.VMEM((1, width), F32),
            pltpu.VMEM((1, tokens), jnp.int32),
            pltpu.VMEM((2, tokens), jnp.int32),
            pltpu.VMEM((2, tokens), F32),
            pltpu.VMEM((tokens, width), BF16),
            pltpu.VMEM((length, QH * HD), BF16),
            pltpu.VMEM((2, length + WINDOW, KVH * HD), BF16),
            pltpu.VMEM((width, 2 * CW), BF16),
            pltpu.VMEM((width, CW), BF16),
            pltpu.VMEM((slots, CW), BF16),
            pltpu.VMEM((ny, slots, CW), BF16),
            pltpu.VMEM((ny, slots, CW), BF16),
            pltpu.VMEM((slots, 2 * CW), F32),
            pltpu.VMEM((slots, CW), F32),
            pltpu.VMEM((slots, CW), BF16),
            pltpu.VMEM((n_ep * CAP, 128), BF16),
            pltpu.VMEM((length, QH * HD), BF16),
            pltpu.VMEM((2, tokens, n_ep * CAP), BF16),
            pltpu.VMEM((2 * WINDOW, 2 * WINDOW), F32),
            pltpu.VMEM((tokens, 8), F32),
            dma((12,)),
            dma((3,)),
            dma((3,)),
            dma((2,)),
            dma((1,)),
            dma((NSUB,)),
            dma((2, 2, steps, NSUB)),
            dma((2, 2, steps, NSUB)),
            dma((2,)),
            dma((1,)),
        ],
        compiler_params=pltpu.CompilerParams(
            collective_id=0, has_side_effects=True, vmem_limit_bytes=66900000
        ),
        name="step",
    )(
        queries,
        keys_values,
        sink_logits,
        moe_rows,
        norm_gain.reshape(1, width),
        group_choice.reshape(1, tokens),
        member_choice.T,
        route_weight.T,
        w_gate,
        w_up,
        w_down,
    )
    return pl.pallas_call(
        hand_on,
        out_shape=(
            jax.ShapeDtypeStruct(attended.shape, BF16),
            jax.ShapeDtypeStruct(mixed.shape, BF16),
        ),
        in_specs=[hbm, hbm],
        out_specs=(hbm, hbm),
        scratch_shapes=[
            pltpu.VMEM(attended.shape, BF16),
            pltpu.VMEM(mixed.shape, BF16),
            dma((2, 5)),
        ],
        compiler_params=pltpu.CompilerParams(vmem_limit_bytes=66900000),
        name="hand_on",
    )(attended, mixed)


def solution(mesh):
    in_specs = (
        P(("ep", "tp"), None),
        P(None, ("ep", "tp"), None),
        P(),
        P("ep", None),
        P(),
        P("ep"),
        P("ep", None),
        P("ep", None),
        P("ep", None, "tp"),
        P("ep", None, "tp"),
        P("ep", None, "tp"),
    )
    out_specs = (P(("ep", "tp"), None), P("ep", "tp"))
    body = functools.partial(shards, mesh.shape["ep"], mesh.shape["tp"])
    return jax.shard_map(body, mesh=mesh, in_specs=in_specs, out_specs=out_specs, check_vma=False)
```

time: 84.3 us -> 76.5 us (0.907)
  local copies, waits for them, and re-layouts: 7.36 us -> 0 us
    unnamed x18 -> x0, local copies, waits for them, and re-layouts: 7.36 us -> none
    pallas_call x0 -> x1, Pallas kernels: none -> 2.01 us  [shards(): pl.pallas_call(hand_on, out_shape=(jax.ShapeDtypeStruct(attended.shape, B...]
    pallas_call x1, Pallas kernels: 75 us -> 73.7 us  [shards(): pl.pallas_call(functools.partial(kernel, n_ep, n_tp), out_shape=(jax.Shap...]
where the time goes in v2:
time: 76.5 us; the launch traced here: 76.4 us
  Pallas kernels  75.7 us (99%)
    pallas_call x1, Pallas kernels, shards(): pl.pallas_call(functools.partial(kernel, n_ep, n_tp), out_shape=(jax.Shap...  73.7 us
    pallas_call x1, Pallas kernels, shards(): pl.pallas_call(hand_on, out_shape=(jax.ShapeDtypeStruct(attended.shape, B...  2.01 us

profile of v2, /device:TPU:1, one launch (start us, length us, event | category | flops | bytes accessed | tf_op | source)
XLA Modules:
  0.0 76.4 jit_solution(17777498935665345689)
XLA Ops:
  0.6 73.7 %step.1 = (bf16[384,1024]{1,0:T(8,128)(2,1)}, bf16[256,128]{1,0:T(8,128)(2,1)}) custom-call(bf16[384,1024]{1,0:T(8,128)(2,1)} %q_hbm.1, bf16[2,384,256]{2,1,0:T(8,128)(2,1)} %kv_hbm.1, f32[16]{0:T(128)} %sink_hbm.1, bf16[256,2048]{1,0:T(8,128)(2,1)} %rows_hbm.1, f32[1,2048]{1,0:T(1,128)} %bitcast.4, s32[1,256]{1,0:T(1,128)} %bitcast.7, s32[2,256]{1,0:T(2,128)} %bitcast.5, ...), custom_call_target="tpu_custom_call" | custom-call | tf_op jit(solution)/shard_map/step/pallas_call | solution.py:501
  74.4 2.0 %hand_on.1 = (bf16[384,1024]{1,0:T(8,128)(2,1)}, bf16[256,128]{1,0:T(8,128)(2,1)}) custom-call(bf16[384,1024]{1,0:T(8,128)(2,1)} %get-tuple-element.4.att_in, bf16[256,128]{1,0:T(8,128)(2,1)} %get-tuple-element.5.mix_in), custom_call_target="tpu_custom_call" | custom-call | tf_op jit(solution)/shard_map/hand_on/pallas_call | solution.py:559

commit v3 on v2

--- a/solution.py
+++ b/solution.py
@@ -48,7 +48,8 @@
     wu_hbm,
     wd_hbm,
     att_out,
-    mix_ref,
+    rbuf,
+    sheet_out,
     sink_ref,
     gain_ref,
     group_ref,
@@ -65,11 +66,9 @@
     acc,
     acc2,
     obuf,
-    rbuf,
     att_v,
-    pick,
     maskb,
-    share,
+    sheet_v,
     loc_sem,
     w_send,
     w_recv,
@@ -145,7 +144,7 @@
         return carry
 
     with jax.named_scope("greet"):
-        lax.fori_loop(1, plane, greet, 0)
+        lax.fori_loop(1, plane, greet, 0, unroll=9 if plane == 64 else 1)
     pl.semaphore_signal(barrier, inc=1, device_id=device(ep, 2 * right + c))
     pl.semaphore_signal(barrier, inc=1, device_id=device(ep, 2 * left + c))
     flat = ep * n_tp + tp
@@ -184,11 +183,14 @@
             part = rows_v[:, i * 128 : (i + 1) * 128].astype(F32)
             square = square + part * part
         mean = jnp.sum(square, axis=1, keepdims=True) * (1.0 / width)
-        columns = pl.ds(pl.multiple_of(y * CW, CW), CW)
-        normed = (
-            rows_v[:, columns].astype(F32) * lax.rsqrt(mean + 1e-06) * gain_ref[:, columns]
-        ).astype(BF16)
-        outb[...] = dot(seats, normed).astype(BF16)
+        scale = lax.rsqrt(mean + 1e-06)
+
+        def seat_rows(k, chunk):
+            columns = pl.ds(pl.multiple_of(chunk * CW, CW), CW)
+            normed = rows_v[:, columns].astype(F32) * scale * gain_ref[:, columns]
+            outb[k] = dot(seats, normed.astype(BF16)).astype(BF16)
+
+        seat_rows(0, y)
 
     with jax.named_scope("barrier"):
         pl.semaphore_wait(barrier, plane - 1 + 4)
@@ -199,20 +201,45 @@
     def block(j):
         return pl.ds(pl.multiple_of(j * HALF, HALF), HALF)
 
-    def dispatch(j, carry):
+    near = steps - 1
+    far = lax.rem(y + steps, ny)
+    ahead = lax.rem(y + near, ny)
+    behind = lax.rem(y + ny - near, ny)
+
+    def hand_over(k, row, chunk, j):
         e = lax.rem(ep + offset(j), n_ep)
         pltpu.make_async_remote_copy(
-            src_ref=outb.at[block(e)],
-            dst_ref=xbuf.at[y, block(j)],
-            send_sem=d_send.at[0],
-            recv_sem=d_recv.at[lax.div(j, per_sub)],
+            src_ref=outb.at[row, block(e)],
+            dst_ref=xbuf.at[chunk, block(j)],
+            send_sem=d_send.at[k],
+            recv_sem=d_recv.at[k, lax.div(j, per_sub)],
             device_id=device(e, tp),
         ).start()
+
+    def dispatch(j, carry):
+        hand_over(0, 0, y, j)
         return carry
+
+    def dispatch_more(j, carry):
+        odd = lax.rem(lax.div(j, per_sub), 2)
+        hand_over(1, 1, far, j)
+        hand_over(2, 2 + odd, lax.rem(y + near + odd * (ny - 2 * near) + ny, ny), j)
+        return carry
+
+    def keep(k, row, chunk):
+        pltpu.make_async_copy(
+            outb.at[row, block(ep)], xbuf.at[chunk, block(0)], d_recv.at[k, 0]
+        ).start()
 
     with jax.named_scope("dispatch"):
         lax.fori_loop(1, n_ep, dispatch, 0)
-        pltpu.make_async_copy(outb.at[block(ep)], xbuf.at[y, block(0)], d_recv.at[0]).start()
+        keep(0, 0, y)
+        seat_rows(1, far)
+        seat_rows(2, ahead)
+        seat_rows(3, behind)
+        lax.fori_loop(1, n_ep, dispatch_more, 0)
+        keep(1, 1, far)
+        keep(2, 2, ahead)
 
     edge = pltpu.make_async_remote_copy(
         src_ref=kv_hbm.at[:, pl.ds(length - WINDOW, WINDOW), :],
@@ -239,16 +266,13 @@
 
     with jax.named_scope("pick"):
         small[3].wait()
-        sheet = [weight_ref[...]]
+        sheet_v[0:2, :] = weight_ref[...]
         for k in range(2):
             seat = jnp.sum(jnp.where(named[k], position, 0.0), axis=0, keepdims=True)
-            sheet.append(chosen[k : k + 1, :].astype(F32) * CAP + seat)
-        sheet.append(jnp.zeros((4, tokens), F32))
-        upright = jnp.concatenate(sheet, axis=0).T
-        share[...] = upright
-        for k in range(2):
-            place = upright[:, 2 + k : 3 + k].astype(jnp.int32)
-            pick[k] = jnp.where(place == iota((tokens, n_ep * CAP), 1), 1.0, 0.0).astype(BF16)
+            sheet_v[2 + k : 3 + k, :] = chosen[k : k + 1, :].astype(F32) * CAP + seat
+        sheet_v[4:8, :] = jnp.zeros((4, tokens), F32)
+        put_sheet = pltpu.make_async_copy(sheet_v, sheet_out, loc_sem.at[12])
+        put_sheet.start()
 
     gap = lax.rem(iota((2 * WINDOW, 2 * WINDOW), 0), WINDOW) + WINDOW - iota((2 * WINDOW, 2 * WINDOW), 1)
     maskb[...] = jnp.where((gap >= 0) & (gap < WINDOW), 0.0, -1e30)
@@ -297,12 +321,14 @@
             for i in range(2):
                 att_v[rows, tiles[i]] = out[i * WINDOW : (i + 1) * WINDOW]
 
-    def attend_tail(i, carry):
-        attend(1 + lax.div(i, 2), lax.rem(i, 2))
-        return carry
-
-    with jax.named_scope("attend"):
-        lax.fori_loop(0, 2 * (blocks - 1), attend_tail, 0)
+    def attend_next(i):
+        if i < 2 * blocks:
+            b, p = (i // 2 + 1) % blocks, i % 2
+            if b == 0 and p == 0:
+                edge.wait_recv()
+            attend(b, p)
+        if i == 2 * blocks - 1:
+            pltpu.make_async_copy(att_v, att_out, loc_sem.at[6]).start()
 
     def piece(buf, phase, way, t, sub, incoming):
         hop = t + 1 if incoming else t
@@ -317,12 +343,16 @@
             device_id=device(ep, 2 * target + c),
         )
 
-    def travels(way, t, sub):
-        return t < steps - 1 or (sub % 2 == 0) == (way == 0)
+    lasts = (steps - 2, steps - 1)
+
+    def travels(phase, way, t, sub):
+        if t == lasts[phase]:
+            return (sub % 2 == 0) == (way == 0)
+        return t < lasts[phase]
 
     def send(buf, phase, t, sub):
         for way in range(2):
-            if travels(way, t, sub):
+            if travels(phase, way, t, sub):
                 piece(buf, phase, way, t, sub, False).start()
 
     def add_chunk(buf, weights, total_ref, chunk, first=False):
@@ -334,27 +364,35 @@
 
     def ring(buf, weights, total_ref, phase, between):
         add_chunk(buf, weights, total_ref, y, True)
-        for t in range(steps - 1):
+        for t in range(lasts[phase]):
             for sub in range(NSUB):
                 for way in range(2):
                     piece(buf, phase, way, t, sub, True).wait_recv()
-                    if travels(way, t + 1, sub):
+                    if travels(phase, way, t + 1, sub):
                         piece(buf, phase, way, t + 1, sub, False).start()
             between(t)
             add_chunk(buf, weights, total_ref, lax.rem(y + ny - t - 1, ny))
             add_chunk(buf, weights, total_ref, lax.rem(y + t + 1, ny))
 
     def last_piece(buf, phase, sub):
-        way = 0 if travels(0, steps - 1, sub) else 1
-        piece(buf, phase, way, steps - 1, sub, True).wait_recv()
-
-    far = lax.rem(y + steps, ny)
-    far_rows = pl.ds(pl.multiple_of(far * CW, CW), CW)
+        way = sub % 2
+        piece(buf, phase, way, lasts[phase], sub, True).wait_recv()
+
+    def rows_of(chunk):
+        return pl.ds(pl.multiple_of(chunk * CW, CW), CW)
+
+    def landed(k, chunk, sub):
+        held = xbuf.at[chunk, pl.ds(sub * sr, sr)]
+        pltpu.make_async_copy(held, held, d_recv.at[k, sub]).wait()
 
     def hide(sub):
+        landed(1, far, sub)
+        landed(2, ahead if sub % 2 == 0 else behind, sub)
         last_piece(xbuf, 0, sub)
         rows = pl.ds(sub * sr, sr)
-        both = acc[rows, :] + dot(xbuf[far, rows], wgu[far_rows, :])
+        both = acc[rows, :]
+        for chunk in (far, ahead, behind):
+            both = both + dot(xbuf[chunk, rows], wgu[rows_of(chunk), :])
         gate = both[:, :CW]
         hbuf[y, rows] = (gate / (1.0 + jnp.exp(-gate)) * both[:, CW:]).astype(BF16)
         send(hbuf, 1, 0, sub)
@@ -393,39 +431,33 @@
     def finish(sub):
         last_piece(hbuf, 1, sub)
         rows = pl.ds(sub * sr, sr)
-        obuf[rows, :] = (acc2[rows, :] + dot(hbuf[far, rows], wd[far_rows, :])).astype(BF16)
+        obuf[rows, :] = (acc2[rows, :] + dot(hbuf[far, rows], wd[rows_of(far), :])).astype(BF16)
         lax.fori_loop(sub * per_sub, (sub + 1) * per_sub, give_back, 0)
 
     def arrive(sub):
-        held = xbuf.at[y, pl.ds(sub * sr, sr)]
-        pltpu.make_async_copy(held, held, d_recv.at[sub]).wait()
+        landed(0, y, sub)
         send(xbuf, 0, 0, sub)
 
-    def early(t):
-        if t == 0:
-            edge.wait_recv()
-        for p in range(2):
-            if t == min(p, steps - 2):
-                attend(0, p)
-        if t == steps - 2:
-            pltpu.make_async_copy(att_v, att_out, loc_sem.at[6]).start()
-
     with jax.named_scope("arrive"):
-        for sub in range(NSUB):
+        arrive(0)
+        for sub in range(1, NSUB):
+            attend_next(sub - 1)
             arrive(sub)
     with jax.named_scope("weights"):
         for i in range(2):
             load_w[i].wait()
             share_w[i].wait_recv()
     with jax.named_scope("ringx"):
-        ring(xbuf, wgu, acc, 0, early)
+        ring(xbuf, wgu, acc, 0, lambda t: attend_next(NSUB - 1 + t))
     with jax.named_scope("middle"):
         for sub in range(NSUB):
             hide(sub)
     load_w[2].wait()
     share_w[2].wait_recv()
     with jax.named_scope("ringh"):
-        ring(hbuf, wd, acc2, 1, lambda t: None)
+        ring(hbuf, wd, acc2, 1, lambda t: attend_next(NSUB - 1 + lasts[0] + t))
+        for i in range(NSUB - 1 + lasts[0] + lasts[1], 2 * blocks):
+            attend_next(i)
     with jax.named_scope("down"):
         for sub in range(NSUB):
             finish(sub)
@@ -435,10 +467,11 @@
             for way in range(2):
                 for t in range(steps):
                     for sub in range(NSUB):
-                        if travels(way, t, sub):
+                        if travels(phase, way, t, sub):
                             piece(buf, phase, way, t, sub, False).wait_send()
-        sent = outb.at[pl.ds(0, slots - HALF)]
-        pltpu.make_async_copy(sent, sent, d_send.at[0]).wait()
+        sent = outb.at[0, pl.ds(0, slots - HALF)]
+        for k in range(3):
+            pltpu.make_async_copy(sent, sent, d_send.at[k]).wait()
         edge.wait_send()
         for copy in share_w:
             copy.wait_send()
@@ -446,33 +479,45 @@
 
     with jax.named_scope("home"):
         pltpu.make_async_copy(rbuf, rbuf, r_recv.at[0]).wait()
-    with jax.named_scope("mix"):
-        mixed = share[:, 0:1] * dot(pick[0], rbuf[...])
-        mixed = mixed + share[:, 1:2] * dot(pick[1], rbuf[...])
-        mix_ref[...] = mixed.astype(BF16)
-
+    put_sheet.wait()
     back = obuf.at[:, pl.ds(0, 128)]
     pltpu.make_async_copy(back, back, r_send.at[0]).wait()
     back_less = obuf.at[pl.ds(0, slots - HALF), pl.ds(0, 128)]
     pltpu.make_async_copy(back_less, back_less, r_send.at[1]).wait()
 
 
-def hand_on(att_in, mix_in, att_out, mix_out, att_v, mix_v, sem):
+def hand_on(att_in, back_in, sheet_in, att_out, mix_out, att_v, back_v, sheet_v, mix_v, sem):
     pieces = 4
     size = att_v.shape[0] // pieces
-    ways = [(mix_in, mix_v, mix_out)]
+    load_sheet = pltpu.make_async_copy(sheet_in, sheet_v, sem.at[0, 4])
+    load_back = pltpu.make_async_copy(back_in, back_v, sem.at[0, 5])
+    load_sheet.start()
+    load_back.start()
+    loads, stores = [], []
     for i in range(pieces):
         part = pl.ds(i * size, size)
-        ways.append((att_in.at[part], att_v.at[part], att_out.at[part]))
-    loads = [pltpu.make_async_copy(a, b, sem.at[0, i]) for i, (a, b, _) in enumerate(ways)]
-    stores = [pltpu.make_async_copy(b, c, sem.at[1, i]) for i, (_, b, c) in enumerate(ways)]
+        loads.append(pltpu.make_async_copy(att_in.at[part], att_v.at[part], sem.at[0, i]))
+        stores.append(pltpu.make_async_copy(att_v.at[part], att_out.at[part], sem.at[1, i]))
     for load in loads:
         load.start()
+    load_sheet.wait()
+    sheet = sheet_v[...].T
+    shape = (sheet.shape[0], back_v.shape[0])
+    picks = [
+        jnp.where(sheet[:, 2 + k : 3 + k].astype(jnp.int32) == iota(shape, 1), 1.0, 0.0).astype(BF16)
+        for k in range(2)
+    ]
+    load_back.wait()
+    mixed = sheet[:, 0:1] * dot(picks[0], back_v[...])
+    mix_v[...] = (mixed + sheet[:, 1:2] * dot(picks[1], back_v[...])).astype(BF16)
+    put = pltpu.make_async_copy(mix_v, mix_out, sem.at[1, 4])
+    put.start()
     for load, store in zip(loads, stores):
         load.wait()
         store.start()
     for store in stores:
         store.wait()
+    put.wait()
 
 
 def shards(
@@ -496,16 +541,16 @@
     ny = n_tp // 2
     steps = ny // 2
     hbm = pl.BlockSpec(memory_space=pl.ANY)
-    vmem = pl.BlockSpec(memory_space=pltpu.VMEM)
     dma = pltpu.SemaphoreType.DMA
-    attended, mixed = pl.pallas_call(
+    attended, returned, sheet = pl.pallas_call(
         functools.partial(kernel, n_ep, n_tp),
         out_shape=(
             jax.ShapeDtypeStruct(queries.shape, BF16),
-            jax.ShapeDtypeStruct((tokens, 128), BF16),
+            jax.ShapeDtypeStruct((n_ep * CAP, 128), BF16),
+            jax.ShapeDtypeStruct((8, tokens), F32),
         ),
         in_specs=[hbm] * 11,
-        out_specs=(hbm, vmem),
+        out_specs=(hbm, hbm, hbm),
         scratch_shapes=[
             pltpu.SMEM((QH,), F32),
             pltpu.VMEM((1, width), F32),
@@ -517,23 +562,21 @@
             pltpu.VMEM((2, length + WINDOW, KVH * HD), BF16),
             pltpu.VMEM((width, 2 * CW), BF16),
             pltpu.VMEM((width, CW), BF16),
-            pltpu.VMEM((slots, CW), BF16),
+            pltpu.VMEM((4, slots, CW), BF16),
             pltpu.VMEM((ny, slots, CW), BF16),
             pltpu.VMEM((ny, slots, CW), BF16),
             pltpu.VMEM((slots, 2 * CW), F32),
             pltpu.VMEM((slots, CW), F32),
             pltpu.VMEM((slots, CW), BF16),
-            pltpu.VMEM((n_ep * CAP, 128), BF16),
             pltpu.VMEM((length, QH * HD), BF16),
-            pltpu.VMEM((2, tokens, n_ep * CAP), BF16),
             pltpu.VMEM((2 * WINDOW, 2 * WINDOW), F32),
-            pltpu.VMEM((tokens, 8), F32),
-            dma((12,)),
+            pltpu.VMEM((8, tokens), F32),
+            dma((13,)),
             dma((3,)),
             dma((3,)),
             dma((2,)),
-            dma((1,)),
-            dma((NSUB,)),
+            dma((3,)),
+            dma((3, NSUB)),
             dma((2, 2, steps, NSUB)),
             dma((2, 2, steps, NSUB)),
             dma((2,)),
@@ -560,18 +603,20 @@
         hand_on,
         out_shape=(
             jax.ShapeDtypeStruct(attended.shape, BF16),
-            jax.ShapeDtypeStruct(mixed.shape, BF16),
+            jax.ShapeDtypeStruct((tokens, 128), BF16),
         ),
-        in_specs=[hbm, hbm],
+        in_specs=[hbm, hbm, hbm],
         out_specs=(hbm, hbm),
         scratch_shapes=[
             pltpu.VMEM(attended.shape, BF16),
-            pltpu.VMEM(mixed.shape, BF16),
-            dma((2, 5)),
+            pltpu.VMEM(returned.shape, BF16),
+            pltpu.VMEM(sheet.shape, F32),
+            pltpu.VMEM((tokens, 128), BF16),
+            dma((2, 6)),
         ],
         compiler_params=pltpu.CompilerParams(vmem_limit_bytes=66900000),
         name="hand_on",
-    )(attended, mixed)
+    )(attended, returned, sheet)
 
 
 def solution(mesh):

time: 76.5 us -> 70.4 us (0.920)
  Pallas kernels: 75.7 us -> 69.6 us
    pallas_call x1, Pallas kernels: 73.7 us -> 67 us  [shards(): pl.pallas_call(functools.partial(kernel, n_ep, n_tp), out_shape=(jax.Shap...]
where the time goes in v3:
time: 70.4 us; the launch traced here: 70.2 us
  Pallas kernels  69.6 us (99%)
    pallas_call x1, Pallas kernels, shards(): pl.pallas_call(functools.partial(kernel, n_ep, n_tp), out_shape=(jax.Shap...  67 us
    pallas_call x1, Pallas kernels, shards(): pl.pallas_call(hand_on, out_shape=(jax.ShapeDtypeStruct(attended.shape, B...  2.55 us

profile of v3, /device:TPU:1, one launch (start us, length us, event | category | flops | bytes accessed | tf_op | source)
XLA Modules:
  0.0 70.2 jit_solution(6808573590344170204)
XLA Ops:
  0.6 67.0 %step.1 = (bf16[384,1024]{1,0:T(8,128)(2,1)}, bf16[1024,128]{1,0:T(8,128)(2,1)}, f32[8,256]{1,0:T(8,128)}) custom-call(bf16[384,1024]{1,0:T(8,128)(2,1)} %q_hbm.1, bf16[2,384,256]{2,1,0:T(8,128)(2,1)} %kv_hbm.1, f32[16]{0:T(128)} %sink_hbm.1, bf16[256,2048]{1,0:T(8,128)(2,1)} %rows_hbm.1, f32[1,2048]{1,0:T(1,128)} %bitcast.4, s32[1,256]{1,0:T(1,128)} %bitcast.7, ...), custom_call_target="tpu_custom_call" | custom-call | tf_op jit(solution)/shard_map/step/pallas_call | solution.py:545
  67.7 2.6 %hand_on.1 = (bf16[384,1024]{1,0:T(8,128)(2,1)}, bf16[256,128]{1,0:T(8,128)(2,1)}) custom-call(bf16[384,1024]{1,0:T(8,128)(2,1)} %get-tuple-element.5.att_in, bf16[1024,128]{1,0:T(8,128)(2,1)} %get-tuple-element.6.back_in, f32[8,256]{1,0:T(8,128)} %get-tuple-element.7.sheet_in), custom_call_target="tpu_custom_call" | custom-call | tf_op jit(solution)/shard_map/hand_on/pallas_call | solution.py:602
